TPU v7x, 32 devices: a whole 2x2x4 slice. The times are simulated.
32 devices in a mesh: ep: 16 (over z, y, x), tp: 2 (over core).
Axes of the slice: x: 2, y: 2, z: 4, core: 2. Of those that a mesh axis runs over, the one named last changes fastest.
Arguments:
- inputs: bfloat16 [1024, 2048], P('ep'), may hold values from -6 to 6
- cache_keys: bfloat16 [1024, 2, 64, 1024], P('ep', 'tp'), may hold values from -6 to 6
- cache_values: bfloat16 [1024, 2, 64, 1024], P('ep', 'tp'), may hold values from -12 to 12
- lengths: int32 [1024], P('ep'), may hold values from 1 to 1024, as said below
- query_weight: bfloat16 [2048, 1024], P(None, 'tp'), may hold values from -0.125 to 0.125
- key_weight: bfloat16 [2048, 128], P(None, 'tp'), may hold values from -0.125 to 0.125
- value_weight: bfloat16 [2048, 128], P(None, 'tp'), may hold values from -0.125 to 0.125
- head_bias: float32 [16], P('tp'), may hold values from -7 to -3
- out_weight: bfloat16 [1024, 2048], P('tp'), may hold values from -0.75 to 0.75
- attend_gain: float32 [2048], replicated, may hold values from 0.1 to 1.9
- router_weight: bfloat16 [2048, 16], replicated, may hold values from -0.125 to 0.125
- routes: int32 [1024, 4], P('ep'), may hold values from 0 to 15, all different within a row; in each aligned block of 64 rows (0 to 63, 64 to 127, ...) at most 32 rows name the same one
- expert_gate: bfloat16 [16, 2048, 512], P('ep', None, 'tp'), may hold values from -0.125 to 0.125
- expert_up: bfloat16 [16, 2048, 512], P('ep', None, 'tp'), may hold values from -0.125 to 0.125
- expert_down: bfloat16 [16, 512, 2048], P('ep', 'tp'), may hold values from -0.25 to 0.25
- shared_gate: bfloat16 [2048, 512], P(None, 'tp'), may hold values from -0.125 to 0.125
- shared_up: bfloat16 [2048, 512], P(None, 'tp'), may hold values from -0.125 to 0.125
- shared_down: bfloat16 [512, 2048], P('tp'), may hold values from -0.25 to 0.25
- final_gain: float32 [2048], P('tp'), may hold values from 0.1 to 1.9
Outputs:
- output: bfloat16 [1024, 2048], P('ep', 'tp')
- new_keys: bfloat16 [1024, 128], P('ep', 'tp')
- new_values: bfloat16 [1024, 128], P('ep', 'tp')
Inputs may be any that keep to these rules, and one draw needn't show every extreme that they name: `lengths`: some sequence has 1024 filled positions and some other has 1. `routes`: each row names 4 different experts. Among the 64 rows of one index of ep no expert is named more than 32 times; some expert is named exactly 32 times by the rows of some index.
All inputs are finite; a program needn't handle non-finite values.
Results may differ from a plain program's by a relative error of at most 0.015.
Values may be sent and summed in bfloat16 or wider, within the bound.
A program may use at most 128 MiB of HBM per device.

v0:
```python
import math
import jax
import jax.numpy as jnp
from jax import lax
from jax.sharding import PartitionSpec as P

RESIDUAL_SCALE = 2.0**0.25
ROUTE_SCALE = 2.5
NORM_EPS = 1e-05


def layer_norm(values, gain_vec):
    row_mean = jnp.mean(values, axis=-1, keepdims=True)
    centered = values - row_mean
    row_var = jnp.mean(centered * centered, axis=-1, keepdims=True)
    return centered * lax.rsqrt(row_var + NORM_EPS) * gain_vec


def strictly_later(size):
    row_pos = lax.broadcasted_iota(jnp.int32, (size, size), 0)
    col_pos = lax.broadcasted_iota(jnp.int32, (size, size), 1)
    return (row_pos > col_pos).astype(jnp.float32)


def later_totals(log_keep):
    lead = log_keep.shape[:-1]
    length = log_keep.shape[-1]
    block_size = math.gcd(length, 128)
    block_count = length // block_size
    blocked = log_keep.reshape(lead + (block_count, block_size))
    inside = jnp.einsum(
        "...bi,ic->...bc", blocked, strictly_later(block_size), precision=lax.Precision.HIGHEST
    )
    block_total = jnp.sum(blocked, axis=-1)
    after = jnp.einsum(
        "...i,ic->...c", block_total, strictly_later(block_count), precision=lax.Precision.HIGHEST
    )
    return (inside + after[..., None]).reshape(lead + (length,))


def on_device(
    inputs,
    cache_keys,
    cache_values,
    lengths,
    query_weight,
    key_weight,
    value_weight,
    head_bias,
    out_weight,
    attend_gain,
    router_weight,
    routes,
    expert_gate,
    expert_up,
    expert_down,
    shared_gate,
    shared_up,
    shared_down,
    final_gain,
):
    seq_count, model_width = inputs.shape
    key_heads, head_size, cache_length = cache_keys.shape[1:]
    query_heads = head_bias.shape[0]
    groups = query_heads // key_heads
    choices_count = routes.shape[1]
    experts = router_weight.shape[1]
    core_index = lax.axis_index("tp")
    half_width = model_width // lax.axis_size("tp")
    query = jnp.dot(inputs, query_weight, preferred_element_type=jnp.float32).astype(jnp.bfloat16)
    query = query.reshape(seq_count, key_heads, groups, head_size)
    new_keys = jnp.dot(inputs, key_weight, preferred_element_type=jnp.float32).astype(jnp.bfloat16)
    new_values = jnp.dot(inputs, value_weight, preferred_element_type=jnp.float32).astype(
        jnp.bfloat16
    )
    scores = jnp.einsum("skgd,skdc->skgc", query, cache_keys, preferred_element_type=jnp.float32)
    scores = scores * head_size ** (-0.5) + head_bias.reshape(key_heads, groups)[None, :, :, None]
    usable = (
        lax.broadcasted_iota(jnp.int32, (1, 1, 1, cache_length), 3) < lengths[:, None, None, None]
    )
    log_keep = jnp.where(usable, jax.nn.log_sigmoid(-scores), 0.0)
    later_sum = later_totals(log_keep)
    stick_weight = jnp.where(usable, jnp.exp(jax.nn.log_sigmoid(scores) + later_sum), 0.0).astype(
        jnp.bfloat16
    )
    attended = jnp.einsum(
        "skgc,skdc->skgd", stick_weight, cache_values, preferred_element_type=jnp.float32
    )
    attended = attended.astype(jnp.bfloat16).reshape(seq_count, query_heads * head_size)
    attention = lax.psum(
        jnp.dot(attended, out_weight, preferred_element_type=jnp.float32).astype(jnp.bfloat16), "tp"
    ).astype(jnp.float32)
    hidden = layer_norm(
        RESIDUAL_SCALE * inputs.astype(jnp.float32) + attention, attend_gain
    ).astype(jnp.bfloat16)
    router_probs = jax.nn.sigmoid(
        jnp.dot(hidden, router_weight, preferred_element_type=jnp.float32)
    )
    picked = routes[:, :, None] == lax.broadcasted_iota(jnp.int32, (1, 1, experts), 2)
    chosen = jnp.sum(jnp.where(picked, router_probs[:, None, :], 0.0), axis=2)
    route_weights = ROUTE_SCALE * chosen / jnp.sum(chosen, axis=1, keepdims=True)
    capacity = 2 * seq_count * choices_count // experts
    row_total = seq_count * choices_count
    onehot_float = picked.reshape(row_total, experts).astype(jnp.float32)
    earlier_count = jnp.dot(
        strictly_later(row_total), onehot_float, precision=lax.Precision.HIGHEST
    )
    slot_index = jnp.sum(earlier_count * onehot_float, axis=1).astype(jnp.int32)
    target = routes.reshape(-1) * capacity + slot_index
    selector_float = (
        target[:, None] == lax.broadcasted_iota(jnp.int32, (1, experts * capacity), 1)
    ).astype(jnp.float32)
    selector = selector_float.astype(jnp.bfloat16)
    placement = jnp.sum(selector_float.reshape(seq_count, choices_count, -1), axis=1).astype(
        jnp.bfloat16
    )
    outgoing = lax.dot_general(
        placement, hidden, (((0,), (0,)), ((), ())), preferred_element_type=jnp.float32
    )
    outgoing = outgoing.astype(jnp.bfloat16).reshape(experts, capacity, -1)
    arrived = lax.all_to_all(outgoing, "ep", split_axis=0, concat_axis=0, tiled=True)
    senders, slot_count, _ = arrived.shape
    flat_rows = arrived.reshape(senders * slot_count, -1)
    gate_act = jnp.dot(flat_rows, expert_gate[0], preferred_element_type=jnp.float32)
    up_act = jnp.dot(flat_rows, expert_up[0], preferred_element_type=jnp.float32)
    inner = (jax.nn.silu(gate_act) * up_act).astype(jnp.bfloat16)
    partial_value = jnp.dot(inner, expert_down[0], preferred_element_type=jnp.float32)
    summed = lax.psum_scatter(
        partial_value.astype(jnp.bfloat16), "tp", scatter_dimension=1, tiled=True
    )
    back_rows = summed.reshape(senders, slot_count, -1)
    returned = lax.all_to_all(back_rows, "ep", split_axis=0, concat_axis=0, tiled=True)
    gathered = jnp.dot(
        selector, returned.reshape(experts * capacity, -1), preferred_element_type=jnp.float32
    )
    gathered = gathered.reshape(seq_count, choices_count, -1)
    routed = jnp.sum(route_weights[:, :, None] * gathered, axis=1)
    shared_g = jnp.dot(hidden, shared_gate, preferred_element_type=jnp.float32)
    shared_u = jnp.dot(hidden, shared_up, preferred_element_type=jnp.float32)
    shared_inner = (jax.nn.silu(shared_g) * shared_u).astype(jnp.bfloat16)
    shared_partial = jnp.dot(shared_inner, shared_down, preferred_element_type=jnp.float32)
    shared_result = lax.psum_scatter(
        shared_partial.astype(jnp.bfloat16), "tp", scatter_dimension=1, tiled=True
    ).astype(jnp.float32)
    own_hidden = lax.dynamic_slice_in_dim(hidden, core_index * half_width, half_width, 1)
    mixed_rows = RESIDUAL_SCALE * own_hidden.astype(jnp.float32) + routed + shared_result
    totals = lax.psum((jnp.sum(mixed_rows, axis=1), jnp.sum(mixed_rows * mixed_rows, axis=1)), "tp")
    row_mean = totals[0] / model_width
    row_var = totals[1] / model_width - row_mean * row_mean
    normed = (mixed_rows - row_mean[:, None]) * lax.rsqrt(row_var + NORM_EPS)[:, None]
    output = (normed * final_gain).astype(jnp.bfloat16)
    return (output, new_keys, new_values)


def solution(mesh):
    placed = (
        P("ep", None),
        P("ep", "tp", None, None),
        P("ep", "tp", None, None),
        P("ep"),
        P(None, "tp"),
        P(None, "tp"),
        P(None, "tp"),
        P("tp"),
        P("tp", None),
        P(),
        P(),
        P("ep", None),
        P("ep", None, "tp"),
        P("ep", None, "tp"),
        P("ep", "tp", None),
        P(None, "tp"),
        P(None, "tp"),
        P("tp", None),
        P("tp"),
    )
    return jax.shard_map(
        on_device,
        mesh=mesh,
        in_specs=placed,
        out_specs=(P("ep", "tp"), P("ep", "tp"), P("ep", "tp")),
        check_vma=False,
    )
```

profile of v0, /device:TPU:9, one launch (start us, length us, event | category | flops | bytes accessed | tf_op | source)
XLA Modules:
  0.0 174.9 jit_solution(5036537996058150898)
XLA Ops:
  7.2 2.3 %convolution_convert_fusion.4 = bf16[64,512]{1,0:T(8,128)(2,1)S(1)} fusion(bf16[64,2048]{1,0:T(8,128)(2,1)} %param.19, bf16[2048,512]{1,0:T(8,128)(2,1)} %param.23), kind=kOutput, calls=%fused_computation.27 | convolution fusion | flops 134250496 | bytes 2424832 | tf_op jit(solution)/shard_map/dot_general | solution.py:70
  9.8 4.6 %fusion.2 = f32[64,8,1024]{2,1,0:T(8,128)S(1)} fusion(bf16[64,8,64]{2,1,0:T(8,128)(2,1)S(1)} %reshape.201, bf16[64,1,64,1024]{3,2,1,0:T(8,128)(2,1)} %param.20), kind=kOutput, calls=%fused_computation.2 | convolution fusion | flops 67108864 | bytes 10551296 | tf_op jit(solution)/shard_map/skgd,skdc->skgc/dot_general | solution.py:76
  14.4 3.0 %fusion.65 = (f32[64,8,8]{1,2,0:T(8,128)S(1)}, f32[64,8,8,128]{3,1,2,0:T(8,128)}) fusion(f32[8]{0:T(128)S(1)} %copy-done.11, f32[64,8,1024]{2,1,0:T(8,128)S(1)} %fusion.2, pred[64,1024]{1,0:T(8,128)(4,1)S(1)} %iota_compare_fusion.3), kind=kLoop, calls=%fused_computation.95 | loop fusion | flops 5763072 | bytes 4276256 | tf_op jit(solution)/shard_map/reduce_sum | solution.py:34
  17.5 0.2 fusion.58
  17.7 0.1 copy.54
  17.8 4.2 %fusion.14 = f32[64,8,8,128]{3,2,1,0:T(8,128)} fusion(f32[64,8,8,128]{3,1,2,0:T(8,128)} %get-tuple-element.11, f32[64,8,8]{2,1,0:T(8,128)S(1)} %copy.54), kind=kOutput, calls=%fused_computation.21 | convolution fusion | flops 805847040 | bytes 4210688 | tf_op jit(solution)/shard_map/...bi,ic->...bc/dot_general | solution.py:31
  22.0 2.7 %reshape.204 = f32[64,8,1024]{2,1,0:T(8,128)} reshape(f32[64,8,8,128]{3,2,1,0:T(8,128)} %fusion.14) | data formatting | bytes 4194304 | tf_op jit(solution)/shard_map/reshape | solution.py:38
  24.7 7.0 %fusion.19 = bf16[64,8,64]{2,1,0:T(8,128)(2,1)S(1)} fusion(bf16[64,1,64,1024]{3,2,1,0:T(8,128)(2,1)} %param.21, f32[64,8,1024]{2,1,0:T(8,128)} %reshape.204, f32[64,8,1024]{2,1,0:T(8,128)} %copy-done.1, f32[8]{0:T(128)S(1)} %copy-done.11, pred[64,1024]{1,0:T(8,128)(4,1)S(1)} %iota_compare_fusion.3), kind=kOutput, calls=%fused_computation.26 | convolution fusion | flops 73957376 | bytes 12714016 | tf_op jit(solution)/shard_map/skgc,skdc->skgd/dot_general | solution.py:86
  31.7 0.1 reshape.206
  31.9 1.2 convolution_convert_fusion.3
  33.4 0.2 fusion.23
  33.9 19.5 %all-reduce.3.cloned.1.call-done = bf16[64,2048]{1,0:T(8,128)(2,1)} async-done(((bf16[64,2048]{1,0:T(8,128)(2,1)}), bf16[64,2048]{1,0:T(8,128)(2,1)}) %all-reduce.3.cloned.1.call-update) | async-done | bytes 262160 | tf_op jit(solution)/shard_map/psum | solution.py:90
  53.4 1.1 fusion.42
  54.5 1.2 multiply_reduce_fusion
  55.7 1.1 multiply_convert_fusion
  56.8 0.7 convolution_convert_fusion.1
  57.6 53.7 %all_to_all.10 = bf16[16,32,2048]{2,1,0:T(8,128)(2,1)S(1)} all-to-all(bf16[16,32,2048]{2,1,0:T(8,128)(2,1)S(1)} %bitcast.62), channel_id=1, replica_groups=mesh['ep'=16,'tp'=2] {'ep'}, dimensions={0} | all-to-all | bytes 4194304 | tf_op jit(solution)/shard_map/all_to_all | solution.py:121
  111.3 1.3 copy-done.3
  112.6 0.7 fusion.31
  113.3 5.8 %convolution_convert_fusion = bf16[512,2048]{1,0:T(8,128)(2,1)} fusion(bf16[512,2048]{1,0:T(8,128)(2,1)} %bitcast.64, bf16[1,256,2048]{2,1,0:T(8,128)(2,1)} %param.33, bf16[1,2048,256]{2,1,0:T(8,128)(2,1)} %param.32, f32[512,256]{1,0:T(8,128)S(1)} %fusion.31), kind=kOutput, calls=%fused_computation.6 | convolution fusion | flops 1075576832 | bytes 6815744 | tf_op jit(solution)/shard_map/dot_general | solution.py:127
  119.2 10.3 %reduce-scatter.3.cloned.1.call-done = bf16[512,1024]{1,0:T(8,128)(2,1)} async-done(((bf16[512,2048]{1,0:T(8,128)(2,1)}), bf16[512,1024]{1,0:T(8,128)(2,1)}) %reduce-scatter.3.cloned.1.call-update) | async-done | bytes 1048592 | tf_op jit(solution)/shard_map/reduce_scatter | solution.py:128
  129.5 6.4 %all-to-all-start.1 = ((bf16[16,32,1024]{2,1,0:T(8,128)(2,1)}), bf16[16,32,1024]{2,1,0:T(8,128)(2,1)}, u32[]{:S(2)}, u32[]{:S(2)}) async-start(bf16[16,32,1024]{2,1,0:T(8,128)(2,1)} %bitcast.65), calls=%async_computation.2 | async-start | bytes 2097152 | tf_op jit(solution)/shard_map/all_to_all | solution.py:132
  135.9 0.8 convolution_convert_fusion.5
  136.8 0.8 convolution_convert_fusion.6
  137.6 1.5 fusion.67
  139.1 3.1 %convolution_convert_fusion.2 = bf16[64,2048]{1,0:T(8,128)(2,1)} fusion(bf16[256,2048]{1,0:T(8,128)(2,1)} %param.36, bf16[64,2048]{1,0:T(8,128)(2,1)S(1)} %multiply_convert_fusion, bf16[2048,256]{1,0:T(8,128)(2,1)} %param.35, f32[64,256]{1,0:T(8,128)S(1)} %fusion.67), kind=kOutput, calls=%fused_computation.8 | convolution fusion | flops 134447104 | bytes 2686976 | tf_op jit(solution)/shard_map/dot_general | solution.py:141
  142.2 0.2 fusion.26
  142.5 17.8 %all-to-all-done.1 = bf16[16,32,1024]{2,1,0:T(8,128)(2,1)} async-done(((bf16[16,32,1024]{2,1,0:T(8,128)(2,1)}), bf16[16,32,1024]{2,1,0:T(8,128)(2,1)}, u32[]{:S(2)}, u32[]{:S(2)}) %all-to-all-start.1) | async-done | bytes 1048608 | tf_op jit(solution)/shard_map/all_to_all | solution.py:132
  160.3 1.7 fusion.17
  162.0 1.1 fusion.64
  163.1 4.5 %all-reduce = (f32[64]{0:T(128)S(1)}, f32[64]{0:T(128)S(1)}) all-reduce(f32[64]{0:T(128)S(1)} %get-tuple-element.4, f32[64]{0:T(128)S(1)} %get-tuple-element.3), channel_id=1, replica_groups=mesh['ep'=16,'tp'=2] {'tp'}, use_global_device_ids=true, to_apply=%region_14.15 | all-reduce | flops 128 | bytes 1024 | tf_op jit(solution)/shard_map/psum | solution.py:147
  167.7 0.8 multiply_convert_fusion.1
  (47 shorter events, 1.2 us)
Async XLA Ops:
  7.2 24.7 %copy-start = (bf16[512,2048]{1,0:T(8,128)(2,1)S(1)}, bf16[512,2048]{1,0:T(8,128)(2,1)}, u32[]{:S(2)}) copy-start(bf16[512,2048]{1,0:T(8,128)(2,1)} %param.27) | copy-start | bytes 6291460
  7.2 2.5 %copy-start.10 = (s32[64]{0:T(128)S(1)}, s32[64]{0:T(128)}, u32[]{:S(2)}) copy-start(s32[64]{0:T(128)} %param.22) | copy-start | bytes 772
  7.2 46.2 %all-reduce.3.cloned.1.call-start = ((), (), s32[]{:S(2)}) async-start(), calls=%async_computation.4 | async-start | bytes 524288 | tf_op jit(solution)/shard_map/psum | solution.py:90
  9.8 4.6 %copy-start.11 = (f32[8]{0:T(128)S(1)}, f32[8]{0:T(128)}, u32[]{:S(2)}) copy-start(f32[8]{0:T(128)} %param.26) | copy-start | bytes 100
  14.4 3.0 %copy-start.1 = (f32[64,8,1024]{2,1,0:T(8,128)}, f32[64,8,1024]{2,1,0:T(8,128)S(1)}, u32[]{:S(2)}) copy-start(f32[64,8,1024]{2,1,0:T(8,128)S(1)} %fusion.2) | copy-start | bytes 6291460
  31.7 1.4 copy-start.7
  31.7 21.6 %copy-start.2 = (bf16[64,2048]{1,0:T(8,128)(2,1)S(1)}, bf16[64,2048]{1,0:T(8,128)(2,1)}, u32[]{:S(2)}) copy-start(bf16[64,2048]{1,0:T(8,128)(2,1)} %param.19) | copy-start | bytes 786436
  31.7 24.0 %copy-start.8 = (f32[2048]{0:T(1024)S(1)}, f32[2048]{0:T(1024)}, u32[]{:S(2)}) copy-start(f32[2048]{0:T(1024)} %param.28) | copy-start | bytes 24580
  33.1 96.4 %reduce-scatter.3.cloned.1.call-start = ((), (), s32[]{:S(2)}) async-start(), calls=%async_computation.5 | async-start | bytes 3145728 | tf_op jit(solution)/shard_map/reduce_scatter | solution.py:128
  57.5 55.0 %copy-start.12 = (bf16[1,2048,256]{2,1,0:T(8,128)(2,1)S(1)}, bf16[1,2048,256]{2,1,0:T(8,128)(2,1)}, u32[]{:S(2)}) copy-start(bf16[1,2048,256]{2,1,0:T(8,128)(2,1)} %param.31) | copy-start | bytes 3145732
  111.3 1.3 copy-start.3
  119.1 16.8 %copy-start.4 = (bf16[2048,64]{0,1:T(8,128)(2,1)S(1)}, bf16[2048,64]{0,1:T(8,128)(2,1)}, u32[]{:S(2)}) copy-start(bf16[2048,64]{0,1:T(8,128)(2,1)} %param.25) | copy-start | bytes 786436
  119.1 17.6 %copy-start.5 = (bf16[2048,64]{0,1:T(8,128)(2,1)S(1)}, bf16[2048,64]{0,1:T(8,128)(2,1)}, u32[]{:S(2)}) copy-start(bf16[2048,64]{0,1:T(8,128)(2,1)} %param.24) | copy-start | bytes 786436
  129.5 30.8 %all-to-all-start.1 = ((bf16[16,32,1024]{2,1,0:T(8,128)(2,1)}), bf16[16,32,1024]{2,1,0:T(8,128)(2,1)}, u32[]{:S(2)}, u32[]{:S(2)}) async-start(bf16[16,32,1024]{2,1,0:T(8,128)(2,1)} %bitcast.65), calls=%async_computation.2 | async-start | bytes 2097152 | tf_op jit(solution)/shard_map/all_to_all | solution.py:132
  135.9 26.1 %reduce-scatter.5.cloned.1.call-start = ((), (), s32[]{:S(2)}) async-start(), calls=%async_computation.6 | async-start | bytes 393216 | tf_op jit(solution)/shard_map/reduce_scatter | solution.py:142
  137.6 4.6 %copy-start.6 = (bf16[2048,16]{0,1:T(8,128)(2,1)S(1)}, bf16[2048,16]{0,1:T(8,128)(2,1)}, u32[]{:S(2)}) copy-start(bf16[2048,16]{0,1:T(8,128)(2,1)} %param.29) | copy-start | bytes 196612
  142.2 25.4 %copy-start.9 = (f32[1024]{0:T(1024)S(1)}, f32[1024]{0:T(1024)}, u32[]{:S(2)}) copy-start(f32[1024]{0:T(1024)} %param.37) | copy-start | bytes 12292
Sparse Core Ops, SparseCore 0:
  33.2 20.0 all-reduce.2
  119.3 10.1 reduce-scatter.2
  142.4 9.5 reduce-scatter.4
where the time goes:
time: 176 us; the launch traced here: 175 us
  blocking collectives  58.3 us (33%)
  waiting for transfers between devices  47.6 us (27%)
  matrix products  35 us (20%)
  between operations  14 us (8%)
  other arithmetic  8.58 us (5%)
  starting transfers between devices  6.54 us (4%)
  local copies, waits for them, and re-layouts  4.99 us (3%)
    all_to_all x1, blocking collectives, on_device(): lax.all_to_all(outgoing, 'ep', split_axis=0, concat_axis=0, tiled=True)  53.7 us
    psum x1, waiting for transfers between devices, on_device(): lax.psum(jnp.dot(attended, out_weight, preferred_element_type=jnp.float32...  19.5 us
    all_to_all x1, waiting for transfers between devices, on_device(): lax.all_to_all(back_rows, 'ep', split_axis=0, concat_axis=0, tiled=True)  17.8 us
    reduce_scatter x1, waiting for transfers between devices, on_device(): lax.psum_scatter(partial_value.astype(jnp.bfloat16), 'tp', scatter_dimens...  10.3 us
    dot_general x1, matrix products, on_device(): jnp.einsum('skgc,skdc->skgd', stick_weight, cache_values, preferred_eleme...  7 us
    all_to_all x1, starting transfers between devices, on_device(): lax.all_to_all(back_rows, 'ep', split_axis=0, concat_axis=0, tiled=True)  6.42 us
    dot_general x1, matrix products, on_device(): jnp.dot(inner, expert_down[0], preferred_element_type=jnp.float32)  5.83 us
    dot_general x1, matrix products, on_device(): jnp.einsum('skgd,skdc->skgc', query, cache_keys, preferred_element_type=j...  4.58 us
  transfers between devices with their start and end apart: 4, of which 3 were waited for; matrix products, arithmetic and copies ran while one was open for 5% of the time, Pallas kernels for 0%

commit v1 on v0

--- a/solution.py
+++ b/solution.py
@@ -87,8 +87,12 @@
         "skgc,skdc->skgd", stick_weight, cache_values, preferred_element_type=jnp.float32
     )
     attended = attended.astype(jnp.bfloat16).reshape(seq_count, query_heads * head_size)
-    attention = lax.psum(
-        jnp.dot(attended, out_weight, preferred_element_type=jnp.float32).astype(jnp.bfloat16), "tp"
+    attention = jnp.sum(
+        lax.all_gather(
+            jnp.dot(attended, out_weight, preferred_element_type=jnp.float32).astype(jnp.bfloat16),
+            "tp",
+        ),
+        axis=0,
     ).astype(jnp.float32)
     hidden = layer_norm(
         RESIDUAL_SCALE * inputs.astype(jnp.float32) + attention, attend_gain

time: 176 us -> 156 us (0.89)
  waiting for transfers between devices: 47.6 us -> 28.1 us
  other arithmetic: 8.58 us -> 5.86 us
  blocking collectives: 58.3 us -> 61 us
    psum x1 -> x0, waiting for transfers between devices: 19.5 us -> none  [on_device(): lax.psum(jnp.dot(attended, out_weight, preferred_element_type=jnp.float32...]
    all_gather x0 -> x1, blocking collectives: none -> 2.48 us  [on_device(): lax.all_gather(jnp.dot(attended, out_weight, preferred_element_type=jnp.f...]
  transfers between devices with their start and end apart: 4 -> 3, of which waited for: 3 -> 2; matrix products, arithmetic and copies ran while one was open for 5% -> 5% of each run, Pallas kernels for 0% -> 0%
where the time goes in v1:
time: 156 us; the launch traced here: 155 us
  blocking collectives  61 us (39%)
  matrix products  34.3 us (22%)
  waiting for transfers between devices  28.1 us (18%)
  between operations  14.3 us (9%)
  starting transfers between devices  6.49 us (4%)
  other arithmetic  5.86 us (4%)
  local copies, waits for them, and re-layouts  5.01 us (3%)
    all_to_all x1, blocking collectives, on_device(): lax.all_to_all(outgoing, 'ep', split_axis=0, concat_axis=0, tiled=True)  54 us
    all_to_all x1, waiting for transfers between devices, on_device(): lax.all_to_all(back_rows, 'ep', split_axis=0, concat_axis=0, tiled=True)  17.7 us
    reduce_scatter x1, waiting for transfers between devices, on_device(): lax.psum_scatter(partial_value.astype(jnp.bfloat16), 'tp', scatter_dimens...  10.3 us
    dot_general x1, matrix products, on_device(): jnp.einsum('skgc,skdc->skgd', stick_weight, cache_values, preferred_eleme...  7 us
    all_to_all x1, starting transfers between devices, on_device(): lax.all_to_all(back_rows, 'ep', split_axis=0, concat_axis=0, tiled=True)  6.41 us
    dot_general x1, matrix products, on_device(): jnp.dot(inner, expert_down[0], preferred_element_type=jnp.float32)  5.83 us
    dot_general x1, matrix products, on_device(): jnp.einsum('skgd,skdc->skgc', query, cache_keys, preferred_element_type=j...  4.58 us
    psum x1, blocking collectives, on_device(): lax.psum((jnp.sum(mixed_rows, axis=1), jnp.sum(mixed_rows * mixed_rows, a...  4.52 us
  transfers between devices with their start and end apart: 3, of which 2 were waited for; matrix products, arithmetic and copies ran while one was open for 5% of the time, Pallas kernels for 0%

profile of v1, /device:TPU:9, one launch (start us, length us, event | category | flops | bytes accessed | tf_op | source)
XLA Modules:
  0.0 155.1 jit_solution(15640398480976909981)
XLA Ops:
  7.2 2.3 %convolution_convert_fusion.4 = bf16[64,512]{1,0:T(8,128)(2,1)S(1)} fusion(bf16[64,2048]{1,0:T(8,128)(2,1)} %param.19, bf16[2048,512]{1,0:T(8,128)(2,1)} %param.23), kind=kOutput, calls=%fused_computation.27 | convolution fusion | flops 134250496 | bytes 2424832 | tf_op jit(solution)/shard_map/dot_general | solution.py:70
  9.8 4.6 %fusion.2 = f32[64,8,1024]{2,1,0:T(8,128)S(1)} fusion(bf16[64,8,64]{2,1,0:T(8,128)(2,1)S(1)} %reshape.201, bf16[64,1,64,1024]{3,2,1,0:T(8,128)(2,1)} %param.20), kind=kOutput, calls=%fused_computation.2 | convolution fusion | flops 67108864 | bytes 10551296 | tf_op jit(solution)/shard_map/skgd,skdc->skgc/dot_general | solution.py:76
  14.4 3.0 %fusion.65 = (f32[64,8,8]{1,2,0:T(8,128)S(1)}, f32[64,8,8,128]{3,1,2,0:T(8,128)}) fusion(f32[8]{0:T(128)S(1)} %copy-done.11, f32[64,8,1024]{2,1,0:T(8,128)S(1)} %fusion.2, pred[64,1024]{1,0:T(8,128)(4,1)S(1)} %iota_compare_fusion.3), kind=kLoop, calls=%fused_computation.95 | loop fusion | flops 5763072 | bytes 4276256 | tf_op jit(solution)/shard_map/reduce_sum | solution.py:34
  17.5 0.2 fusion.58
  17.7 0.1 copy.54
  17.8 4.2 %fusion.14 = f32[64,8,8,128]{3,2,1,0:T(8,128)} fusion(f32[64,8,8,128]{3,1,2,0:T(8,128)} %get-tuple-element.11, f32[64,8,8]{2,1,0:T(8,128)S(1)} %copy.54), kind=kOutput, calls=%fused_computation.21 | convolution fusion | flops 805847040 | bytes 4210688 | tf_op jit(solution)/shard_map/...bi,ic->...bc/dot_general | solution.py:31
  22.0 2.7 %reshape.204 = f32[64,8,1024]{2,1,0:T(8,128)} reshape(f32[64,8,8,128]{3,2,1,0:T(8,128)} %fusion.14) | data formatting | bytes 4194304 | tf_op jit(solution)/shard_map/reshape | solution.py:38
  24.7 7.0 %fusion.19 = bf16[64,8,64]{2,1,0:T(8,128)(2,1)S(1)} fusion(bf16[64,1,64,1024]{3,2,1,0:T(8,128)(2,1)} %param.21, f32[64,8,1024]{2,1,0:T(8,128)} %reshape.204, f32[64,8,1024]{2,1,0:T(8,128)} %copy-done.1, f32[8]{0:T(128)S(1)} %copy-done.11, pred[64,1024]{1,0:T(8,128)(4,1)S(1)} %iota_compare_fusion.3), kind=kOutput, calls=%fused_computation.26 | convolution fusion | flops 73957376 | bytes 12714016 | tf_op jit(solution)/shard_map/skgc,skdc->skgd/dot_general | solution.py:86
  31.7 0.1 reshape.206
  31.9 0.5 convolution_convert_fusion.3
  32.4 2.5 %all-gather = bf16[128,2048]{1,0:T(8,128)(2,1)S(1)} all-gather(bf16[64,2048]{1,0:T(8,128)(2,1)S(1)} %convolution_convert_fusion.3), channel_id=2, replica_groups=mesh['ep'=16,'tp'=2] {'tp'}, dimensions={0}, use_global_device_ids=true | all-gather | bytes 786432 | tf_op jit(solution)/shard_map/all_gather | solution.py:91
  35.0 0.2 fusion.42
  35.2 0.2 multiply_reduce_fusion
  35.7 0.2 fusion.23
  36.2 0.1 multiply_convert_fusion
  36.4 0.7 convolution_convert_fusion.1
  37.1 54.0 %all_to_all.10 = bf16[16,32,2048]{2,1,0:T(8,128)(2,1)S(1)} all-to-all(bf16[16,32,2048]{2,1,0:T(8,128)(2,1)S(1)} %bitcast.63), channel_id=1, replica_groups=mesh['ep'=16,'tp'=2] {'ep'}, dimensions={0} | all-to-all | bytes 4194304 | tf_op jit(solution)/shard_map/all_to_all | solution.py:125
  91.1 1.3 copy-done.3
  92.4 0.7 fusion.31
  93.1 5.8 %convolution_convert_fusion = bf16[512,2048]{1,0:T(8,128)(2,1)} fusion(bf16[512,2048]{1,0:T(8,128)(2,1)} %bitcast.65, bf16[1,256,2048]{2,1,0:T(8,128)(2,1)} %param.33, bf16[1,2048,256]{2,1,0:T(8,128)(2,1)} %param.32, f32[512,256]{1,0:T(8,128)S(1)} %fusion.31), kind=kOutput, calls=%fused_computation.6 | convolution fusion | flops 1075576832 | bytes 6815744 | tf_op jit(solution)/shard_map/dot_general | solution.py:131
  98.9 10.3 %reduce-scatter.3.cloned.1.call-done = bf16[512,1024]{1,0:T(8,128)(2,1)} async-done(((bf16[512,2048]{1,0:T(8,128)(2,1)}), bf16[512,1024]{1,0:T(8,128)(2,1)}) %reduce-scatter.3.cloned.1.call-update) | async-done | bytes 1048592 | tf_op jit(solution)/shard_map/reduce_scatter | solution.py:132
  109.3 6.4 %all-to-all-start.1 = ((bf16[16,32,1024]{2,1,0:T(8,128)(2,1)}), bf16[16,32,1024]{2,1,0:T(8,128)(2,1)}, u32[]{:S(2)}, u32[]{:S(2)}) async-start(bf16[16,32,1024]{2,1,0:T(8,128)(2,1)} %bitcast.67), calls=%async_computation.2 | async-start | bytes 2097152 | tf_op jit(solution)/shard_map/all_to_all | solution.py:136
  115.8 1.6 %fusion.67 = f32[64,256]{1,0:T(8,128)S(1)} fusion(bf16[64,2048]{1,0:T(8,128)(2,1)S(1)} %multiply_convert_fusion, bf16[2048,256]{1,0:T(8,128)(2,1)} %param.34), kind=kOutput, calls=%fused_computation.96 | convolution fusion | flops 67108864 | bytes 1376256 | tf_op jit(solution)/shard_map/dot_general | solution.py:142
  117.3 3.1 %convolution_convert_fusion.2 = bf16[64,2048]{1,0:T(8,128)(2,1)} fusion(bf16[256,2048]{1,0:T(8,128)(2,1)} %param.36, bf16[64,2048]{1,0:T(8,128)(2,1)S(1)} %multiply_convert_fusion, bf16[2048,256]{1,0:T(8,128)(2,1)} %param.35, f32[64,256]{1,0:T(8,128)S(1)} %fusion.67), kind=kOutput, calls=%fused_computation.8 | convolution fusion | flops 134447104 | bytes 2686976 | tf_op jit(solution)/shard_map/dot_general | solution.py:145
  120.5 0.2 fusion.26
  120.7 0.8 convolution_convert_fusion.5
  121.5 0.8 convolution_convert_fusion.6
  122.4 17.7 %all-to-all-done.1 = bf16[16,32,1024]{2,1,0:T(8,128)(2,1)} async-done(((bf16[16,32,1024]{2,1,0:T(8,128)(2,1)}), bf16[16,32,1024]{2,1,0:T(8,128)(2,1)}, u32[]{:S(2)}, u32[]{:S(2)}) %all-to-all-start.1) | async-done | bytes 1048608 | tf_op jit(solution)/shard_map/all_to_all | solution.py:136
  140.1 1.7 %fusion.17 = f32[64,1024]{1,0:T(8,128)S(1)} fusion(bf16[512,1024,1]{1,0,2:T(8,128)(2,1)} %bitcast.15, f32[64,4]{0,1:T(4,128)S(1)} %multiply_divide_fusion, s32[64,4]{0,1:T(4,128)S(1)} %multiply_add_fusion.1), kind=kOutput, calls=%fused_computation.23 | convolution fusion | flops 269287424 | bytes 1312768 | tf_op jit(solution)/shard_map/dot_general | solution.py:137
  141.8 1.1 fusion.64
  142.9 4.5 %all-reduce = (f32[64]{0:T(128)S(1)}, f32[64]{0:T(128)S(1)}) all-reduce(f32[64]{0:T(128)S(1)} %get-tuple-element.4, f32[64]{0:T(128)S(1)} %get-tuple-element.3), channel_id=1, replica_groups=mesh['ep'=16,'tp'=2] {'tp'}, use_global_device_ids=true, to_apply=%region_14.15 | all-reduce | flops 128 | bytes 1024 | tf_op jit(solution)/shard_map/psum | solution.py:151
  147.5 0.8 multiply_convert_fusion.1
  (46 shorter events, 1.3 us)
Async XLA Ops:
  7.2 24.7 %copy-start = (bf16[512,2048]{1,0:T(8,128)(2,1)S(1)}, bf16[512,2048]{1,0:T(8,128)(2,1)}, u32[]{:S(2)}) copy-start(bf16[512,2048]{1,0:T(8,128)(2,1)} %param.27) | copy-start | bytes 6291460
  7.2 2.5 %copy-start.10 = (s32[64]{0:T(128)S(1)}, s32[64]{0:T(128)}, u32[]{:S(2)}) copy-start(s32[64]{0:T(128)} %param.22) | copy-start | bytes 772
  7.2 102.1 %reduce-scatter.3.cloned.1.call-start = ((), (), s32[]{:S(2)}) async-start(), calls=%async_computation.4 | async-start | bytes 3145728 | tf_op jit(solution)/shard_map/reduce_scatter | solution.py:132
  9.8 4.6 %copy-start.11 = (f32[8]{0:T(128)S(1)}, f32[8]{0:T(128)}, u32[]{:S(2)}) copy-start(f32[8]{0:T(128)} %param.26) | copy-start | bytes 100
  14.4 3.0 %copy-start.1 = (f32[64,8,1024]{2,1,0:T(8,128)}, f32[64,8,1024]{2,1,0:T(8,128)S(1)}, u32[]{:S(2)}) copy-start(f32[64,8,1024]{2,1,0:T(8,128)S(1)} %fusion.2) | copy-start | bytes 6291460
  31.7 3.3 %copy-start.2 = (bf16[64,2048]{1,0:T(8,128)(2,1)S(1)}, bf16[64,2048]{1,0:T(8,128)(2,1)}, u32[]{:S(2)}) copy-start(bf16[64,2048]{1,0:T(8,128)(2,1)} %param.19) | copy-start | bytes 786436
  31.9 3.6 %copy-start.7 = (s32[64,4]{0,1:T(4,128)S(1)}, s32[64,4]{0,1:T(4,128)}, u32[]{:S(2)}) copy-start(s32[64,4]{0,1:T(4,128)} %param.30) | copy-start | bytes 3076
  31.9 4.3 %copy-start.8 = (f32[2048]{0:T(1024)S(1)}, f32[2048]{0:T(1024)}, u32[]{:S(2)}) copy-start(f32[2048]{0:T(1024)} %param.28) | copy-start | bytes 24580
  37.1 55.3 %copy-start.12 = (bf16[1,2048,256]{2,1,0:T(8,128)(2,1)S(1)}, bf16[1,2048,256]{2,1,0:T(8,128)(2,1)}, u32[]{:S(2)}) copy-start(bf16[1,2048,256]{2,1,0:T(8,128)(2,1)} %param.31) | copy-start | bytes 3145732
  91.1 1.3 copy-start.3
  109.3 30.8 %all-to-all-start.1 = ((bf16[16,32,1024]{2,1,0:T(8,128)(2,1)}), bf16[16,32,1024]{2,1,0:T(8,128)(2,1)}, u32[]{:S(2)}, u32[]{:S(2)}) async-start(bf16[16,32,1024]{2,1,0:T(8,128)(2,1)} %bitcast.67), calls=%async_computation.2 | async-start | bytes 2097152 | tf_op jit(solution)/shard_map/all_to_all | solution.py:136
  115.7 4.8 %copy-start.6 = (bf16[2048,16]{0,1:T(8,128)(2,1)S(1)}, bf16[2048,16]{0,1:T(8,128)(2,1)}, u32[]{:S(2)}) copy-start(bf16[2048,16]{0,1:T(8,128)(2,1)} %param.29) | copy-start | bytes 196612
  115.7 5.0 %copy-start.4 = (bf16[2048,64]{0,1:T(8,128)(2,1)S(1)}, bf16[2048,64]{0,1:T(8,128)(2,1)}, u32[]{:S(2)}) copy-start(bf16[2048,64]{0,1:T(8,128)(2,1)} %param.25) | copy-start | bytes 786436
  115.7 26.1 %reduce-scatter.5.cloned.1.call-start = ((), (), s32[]{:S(2)}) async-start(), calls=%async_computation.5 | async-start | bytes 393216 | tf_op jit(solution)/shard_map/reduce_scatter | solution.py:146
  117.3 4.2 %copy-start.5 = (bf16[2048,64]{0,1:T(8,128)(2,1)S(1)}, bf16[2048,64]{0,1:T(8,128)(2,1)}, u32[]{:S(2)}) copy-start(bf16[2048,64]{0,1:T(8,128)(2,1)} %param.24) | copy-start | bytes 786436
  120.5 27.0 %copy-start.9 = (f32[1024]{0:T(1024)S(1)}, f32[1024]{0:T(1024)}, u32[]{:S(2)}) copy-start(f32[1024]{0:T(1024)} %param.37) | copy-start | bytes 12292
Sparse Core Ops, SparseCore 0:
  99.1 10.1 reduce-scatter.2
  120.6 9.5 reduce-scatter.4
